TPU v7x, 512 devices: a whole 4x4x16 slice. The times are simulated.
512 devices in a mesh: fs: 16 (over y, x), tp: 32 (over z, core).
Axes of the slice: x: 4, y: 4, z: 16, core: 2. Of those that a mesh axis runs over, the one named last changes fastest.
Arguments:
- saved_input: bfloat16 [16384, 4096], P('fs', 'tp'), may hold values from -6 to 6
- query_cot: bfloat16 [16384, 4096], P('fs', 'tp'), may hold values from -6 to 6
- key_cot: bfloat16 [16384, 4096], P('fs', 'tp'), may hold values from -6 to 6
- query_master: float32 [4096, 4096], P('fs', 'tp'), may hold values from -0.09375 to 0.09375
- key_master: float32 [4096, 4096], P('fs', 'tp'), may hold values from -0.09375 to 0.09375
- query_basis: bfloat16 [4096, 256], P('fs'), may hold values from -3 to 3
- key_basis: bfloat16 [4096, 256], P('fs'), may hold values from -3 to 3
- query_first: float32 [256, 4096], P('fs', 'tp'), may hold values from -240 to 240
- query_second: float32 [256, 4096], P('fs', 'tp'), may hold values from 1000 to 20000
- key_first: float32 [256, 4096], P('fs', 'tp'), may hold values from -240 to 240
- key_second: float32 [256, 4096], P('fs', 'tp'), may hold values from 1000 to 20000
Outputs:
- query_step: float32 [4096, 4096], P('fs', 'tp')
- query_weight: float32 [4096, 4096], P('fs', 'tp')
- query_copy: bfloat16 [4096, 4096], P(None, 'tp')
- query_first_new: float32 [256, 4096], P('fs', 'tp')
- query_second_new: float32 [256, 4096], P('fs', 'tp')
- key_step: float32 [4096, 4096], P('fs', 'tp')
- key_weight: float32 [4096, 4096], P('fs', 'tp')
- key_copy: bfloat16 [4096, 4096], P(None, 'tp')
- key_first_new: float32 [256, 4096], P('fs', 'tp')
- key_second_new: float32 [256, 4096], P('fs', 'tp')
All inputs are finite; a program needn't handle non-finite values.
Results may differ from a plain program's by a relative error of at most 0.0065.
Values may be sent and summed in bfloat16 or wider, within the bound.
A program may use at most 64 MiB of HBM per device.

v0:
```python
import jax
import jax.numpy as jnp
from jax import lax
from jax.sharding import Mesh
from jax.sharding import PartitionSpec as P

D = 4096
HD = 128
FS = ("fs_0", "fs_1")
moment_decay = 0.8
square_decay = 0.9
square_floor = 1.0
norm_floor = 0.01
step_rate = 0.01


def in_one_piece(arrays, axis, dim, along):
    widths = [a.shape[along] for a in arrays]
    both = jnp.concatenate(arrays, axis=along)
    out = lax.all_gather(both, axis, axis=dim, tiled=True)
    return tuple(jnp.split(out, [sum(widths[:k]) for k in range(1, len(widths))], axis=along))


def cut_along(x, dim, count):
    lengths = x.shape
    pieces = x.reshape(*lengths[:dim], count, lengths[dim] // count, *lengths[dim + 1 :])
    return jnp.moveaxis(pieces, dim, 0)


def sent_and_summed(x, axis, dim):
    count = lax.axis_size(axis)
    pieces = lax.all_to_all(cut_along(x, dim, count), axis, 0, 0, tiled=True)
    return jnp.sum(pieces, axis=0)


def sent_to_all(x, axis):
    count = lax.axis_size(axis)
    return lax.all_to_all(jnp.broadcast_to(x[None], (count, *x.shape)), axis, 0, 0, tiled=True)


def in_order(pieces, dim):
    lengths = list(pieces.shape[1:])
    lengths[dim] *= pieces.shape[0]
    return jnp.moveaxis(pieces, 0, dim).reshape(lengths)


def gathered_copies(x, axis, dim):
    pieces = sent_to_all(x, axis)
    return in_order(pieces, dim)


def by_axis(x, axes):
    for axis in axes:
        x = lax.psum(x, axis)
    return x


def split_product(low_part, cot_part):
    upper = low_part.astype(jnp.bfloat16)
    lower = (low_part - upper.astype(jnp.float32)).astype(jnp.bfloat16)
    return jnp.dot(upper.T, cot_part, preferred_element_type=jnp.float32) + jnp.dot(
        lower.T, cot_part, preferred_element_type=jnp.float32
    )


def cot_rows(query_low, key_low, cot_wide, width):

    def low_rows(start, count):
        return jnp.concatenate(
            [
                split_product(query_low, cot_wide[:, :width]),
                split_product(key_low, cot_wide[:, width:]),
            ],
            axis=1,
        )

    return low_rows


def head_squares(update):
    by_head = update.reshape(update.shape[0], -1, HD)
    return jnp.sum(by_head * by_head, axis=(0, 2))


def apply_scale(update, total):
    scale = 1.0 / jnp.sqrt(total / (D * HD) + norm_floor)
    by_head = update.reshape(update.shape[0], -1, HD)
    return (by_head * scale[None, :, None]).reshape(update.shape)


def body(
    saved_input,
    query_cot,
    key_cot,
    query_master,
    key_master,
    query_basis,
    key_basis,
    query_first,
    query_second,
    key_first,
    key_second,
):
    width = query_cot.shape[1]
    low_count = query_first.shape[0]
    cotangents = jnp.concatenate([query_cot, key_cot], axis=1)
    inputs = lax.all_gather(saved_input, "tp", axis=1, tiled=True)
    bases = in_one_piece((query_basis, key_basis), FS, 0, 1)
    query_low = jnp.dot(inputs, bases[0], preferred_element_type=jnp.float32)
    key_low = jnp.dot(inputs, bases[1], preferred_element_type=jnp.float32)
    low_rows = cot_rows(query_low, key_low, cotangents, width)
    projected = sent_and_summed(low_rows(jnp.int32(0), low_count * lax.axis_size(FS)), FS, 0)
    firsts = jnp.concatenate([query_first, key_first], axis=1)
    seconds = jnp.concatenate([query_second, key_second], axis=1)
    first_new = moment_decay * firsts + (1.0 - moment_decay) * projected
    second_new = square_decay * seconds + (1.0 - square_decay) * projected * projected
    ratio = (first_new / jnp.sqrt(second_new + square_floor)).astype(jnp.bfloat16)
    piece = gathered_copies(ratio, FS, 0)
    query_update = jnp.dot(query_basis, piece[:, :width], preferred_element_type=jnp.float32)
    key_update = jnp.dot(key_basis, piece[:, width:], preferred_element_type=jnp.float32)
    query_total, key_total = (
        by_axis(head_squares(query_update), FS),
        by_axis(head_squares(key_update), FS),
    )
    query_step = apply_scale(query_update, query_total)
    key_step = apply_scale(key_update, key_total)
    query_weight = query_master - step_rate * query_step
    key_weight = key_master - step_rate * key_step
    copies = in_one_piece(
        (query_weight.astype(jnp.bfloat16), key_weight.astype(jnp.bfloat16)), FS, 0, 1
    )
    return (
        query_step,
        query_weight,
        copies[0],
        first_new[:, :width],
        second_new[:, :width],
        key_step,
        key_weight,
        copies[1],
        first_new[:, width:],
        second_new[:, width:],
    )


def solution(mesh):
    torus = Mesh(mesh.devices.reshape(4, 4, mesh.shape["tp"]), ("fs_0", "fs_1", "tp"))
    in_specs = (
        P(FS, "tp"),
        P(FS, "tp"),
        P(FS, "tp"),
        P(FS, "tp"),
        P(FS, "tp"),
        P(FS, None),
        P(FS, None),
        P(FS, "tp"),
        P(FS, "tp"),
        P(FS, "tp"),
        P(FS, "tp"),
    )
    out_specs = (
        P(FS, "tp"),
        P(FS, "tp"),
        P(None, "tp"),
        P(FS, "tp"),
        P(FS, "tp"),
        P(FS, "tp"),
        P(FS, "tp"),
        P(None, "tp"),
        P(FS, "tp"),
        P(FS, "tp"),
    )
    return jax.shard_map(body, mesh=torus, in_specs=in_specs, out_specs=out_specs, check_vma=False)
```

profile of v0, /device:TPU:2, one launch (start us, length us, event | category | flops | bytes accessed | tf_op | source)
XLA Modules:
  0.0 306.8 jit_solution(4869370095504522026)
XLA Ops:
  7.2 1.7 pad_maximum_fusion
  9.0 0.7 all-gather.6.cloned.1.call-update
  9.7 73.1 %all-gather.4.cloned.1.call-done = bf16[4096,512]{1,0:T(8,128)(2,1)} async-done(((bf16[256,512]{1,0:T(8,128)(2,1)}), bf16[4096,512]{1,0:T(8,128)(2,1)}) %all-gather.4.cloned.1.call-update) | async-done | bytes 4194320 | tf_op jit(solution)/shard_map/all_gather | solution.py:20
  82.8 97.5 %all-gather.6.cloned.1.call-done = bf16[1024,4096]{1,0:T(8,128)(2,1)} async-done(((bf16[1024,128]{1,0:T(8,128)(2,1)}), bf16[1024,4096]{1,0:T(8,128)(2,1)}) %all-gather.6.cloned.1.call-update) | async-done | bytes 8388624 | tf_op jit(solution)/shard_map/all_gather | solution.py:107
  180.2 6.5 %fusion.4 = f32[1024,256]{0,1:T(8,128)S(1)} fusion(bf16[1024,4096]{1,0:T(8,128)(2,1)} %all-gather.6.cloned.1.call-done, bf16[4096,512]{1,0:T(8,128)(2,1)} %all-gather.4.cloned.1.call-done), kind=kOutput, calls=%fused_computation.4 | convolution fusion | flops 2147483648 | bytes 11534336 | tf_op jit(solution)/shard_map/dot_general | solution.py:109
  186.8 0.3 fusion.14
  187.1 0.3 convolution_add_fusion.1
  187.5 0.4 copy-done.11
  187.8 2.4 fusion.7
  190.3 0.3 fusion.11
  190.7 0.3 convolution_add_fusion
  191.0 0.1 copy.29
  191.1 14.8 %all_to_all.10 = f32[16,16,256]{2,1,0:T(8,128)S(1)} all-to-all(f32[16,16,256]{2,1,0:T(8,128)S(1)} %bitcast.24), channel_id=1, replica_groups=mesh['fs_0'=4,'fs_1'=4,'tp'=32] {'fs_0','fs_1'}, dimensions={0} | all-to-all | bytes 524288 | tf_op jit(solution)/shard_map/all_to_all | solution.py:32
  206.0 0.7 broadcast_in_dim.2
  206.7 4.8 %all-to-all-start.1 = ((bf16[16,16,256]{2,1,0:T(8,128)(2,1)}), bf16[16,16,256]{2,1,0:T(8,128)(2,1)S(1)}, u32[]{:S(2)}, u32[]{:S(2)}) async-start(bf16[16,16,256]{2,1,0:T(8,128)(2,1)} %broadcast_in_dim.2), calls=%async_computation.1 | async-start | bytes 262144 | tf_op jit(solution)/shard_map/all_to_all | solution.py:38
  211.5 0.1 copy.30
  211.6 0.1 copy.31
  211.7 6.4 %all-to-all-done.1 = bf16[16,16,256]{2,1,0:T(8,128)(2,1)S(1)} async-done(((bf16[16,16,256]{2,1,0:T(8,128)(2,1)}), bf16[16,16,256]{2,1,0:T(8,128)(2,1)S(1)}, u32[]{:S(2)}, u32[]{:S(2)}) %all-to-all-start.1) | async-done | bytes 131104 | tf_op jit(solution)/shard_map/all_to_all | solution.py:38
  218.2 0.8 multiply_reduce_fusion.1
  219.0 0.8 multiply_reduce_fusion
  219.8 9.2 %all-reduce.1 = (f32[1]{0:T(128)}, f32[1]{0:T(128)}) all-reduce(f32[1]{0:T(128)} %bitcast.4, f32[1]{0:T(128)} %bitcast.7), channel_id=1, replica_groups=mesh['fs_0'=4,'fs_1'=4,'tp'=32] {'fs_0'}, use_global_device_ids=true, to_apply=%region_2.0 | all-reduce | flops 2 | bytes 16 | tf_op jit(solution)/shard_map/psum | solution.py:54
  229.0 9.8 %all-reduce = (f32[1]{0:T(128)}, f32[1]{0:T(128)}) all-reduce(f32[1]{0:T(128)} %get-tuple-element.32, f32[1]{0:T(128)} %get-tuple-element.33), channel_id=1, replica_groups=mesh['fs_0'=4,'fs_1'=4,'tp'=32] {'fs_1'}, use_global_device_ids=true, to_apply=%region_3.0 | all-reduce | flops 2 | bytes 16 | tf_op jit(solution)/shard_map/psum | solution.py:54
  240.2 0.7 pad_maximum_fusion.2
  240.9 0.6 fusion.27
  241.5 0.8 copy.32
  242.3 0.8 copy.33
  243.1 0.8 copy.35
  243.8 0.8 copy.36
  244.6 51.4 %all-gather.8.cloned.1.call-done = bf16[4096,256]{0,1:T(8,128)(2,1)} async-done(((bf16[256,256]{0,1:T(8,128)(2,1)}), bf16[4096,256]{0,1:T(8,128)(2,1)}) %all-gather.8.cloned.1.call-update) | async-done | bytes 2097168 | tf_op jit(solution)/shard_map/all_gather | solution.py:20
  296.0 1.7 fusion.26
  297.6 1.3 copy.34
  299.0 1.3 copy.37
  (32 shorter events, 0.3 us)
Async XLA Ops:
  7.2 179.6 %copy-start = (bf16[1024,128]{1,0:T(8,128)(2,1)S(1)}, bf16[1024,128]{1,0:T(8,128)(2,1)}, u32[]{:S(2)}) copy-start(bf16[1024,128]{1,0:T(8,128)(2,1)} %param.12) | copy-start | bytes 786436
  7.2 75.6 %all-gather.4.cloned.1.call-start = ((), (), s32[]{:S(2)}) async-start(), calls=%async_computation.2 | async-start | bytes 4456448 | tf_op jit(solution)/shard_map/all_gather | solution.py:20
  9.0 171.3 %all-gather.6.cloned.1.call-start = ((), (), s32[]{:S(2)}) async-start(), calls=%async_computation.3 | async-start | bytes 8650752 | tf_op jit(solution)/shard_map/all_gather | solution.py:107
  180.2 7.2 %copy-start.10 = (bf16[1024,4096]{1,0:T(8,128)(2,1)S(1)}, bf16[1024,4096]{1,0:T(8,128)(2,1)}, u32[]{:S(2)}) copy-start(bf16[1024,4096]{1,0:T(8,128)(2,1)} %all-gather.6.cloned.1.call-done) | copy-start | bytes 25165828
  180.2 7.6 %copy-start.11 = (bf16[4096,512]{1,0:T(8,128)(2,1)S(1)}, bf16[4096,512]{1,0:T(8,128)(2,1)}, u32[]{:S(2)}) copy-start(bf16[4096,512]{1,0:T(8,128)(2,1)} %all-gather.4.cloned.1.call-done) | copy-start | bytes 12582916
  187.8 2.4 copy-start.1
  190.2 15.7 %copy-start.6 = (f32[16,128]{1,0:T(8,128)S(1)}, f32[16,128]{1,0:T(8,128)}, u32[]{:S(2)}) copy-start(f32[16,128]{1,0:T(8,128)} %param.21) | copy-start | bytes 24580
  190.2 15.7 %copy-start.7 = (f32[16,128]{1,0:T(8,128)S(1)}, f32[16,128]{1,0:T(8,128)}, u32[]{:S(2)}) copy-start(f32[16,128]{1,0:T(8,128)} %param.19) | copy-start | bytes 24580
  190.3 15.7 %copy-start.8 = (f32[16,128]{1,0:T(8,128)S(1)}, f32[16,128]{1,0:T(8,128)}, u32[]{:S(2)}) copy-start(f32[16,128]{1,0:T(8,128)} %param.20) | copy-start | bytes 24580
  190.3 15.7 %copy-start.9 = (f32[16,128]{1,0:T(8,128)S(1)}, f32[16,128]{1,0:T(8,128)}, u32[]{:S(2)}) copy-start(f32[16,128]{1,0:T(8,128)} %param.18) | copy-start | bytes 24580
  190.3 21.2 %copy-start.4 = (f32[256,128]{1,0:T(8,128)S(1)}, f32[256,128]{1,0:T(8,128)}, u32[]{:S(2)}) copy-start(f32[256,128]{1,0:T(8,128)} %param.14) | copy-start | bytes 393220
  190.3 21.3 %copy-start.5 = (f32[256,128]{1,0:T(8,128)S(1)}, f32[256,128]{1,0:T(8,128)}, u32[]{:S(2)}) copy-start(f32[256,128]{1,0:T(8,128)} %param.15) | copy-start | bytes 393220
  190.3 27.9 %copy-start.2 = (bf16[256,256]{1,0:T(8,128)(2,1)S(1)}, bf16[256,256]{1,0:T(8,128)(2,1)}, u32[]{:S(2)}) copy-start(bf16[256,256]{1,0:T(8,128)(2,1)} %param.16) | copy-start | bytes 393220
  190.3 28.7 %copy-start.3 = (bf16[256,256]{1,0:T(8,128)(2,1)S(1)}, bf16[256,256]{1,0:T(8,128)(2,1)}, u32[]{:S(2)}) copy-start(bf16[256,256]{1,0:T(8,128)(2,1)} %param.17) | copy-start | bytes 393220
  206.7 11.5 %all-to-all-start.1 = ((bf16[16,16,256]{2,1,0:T(8,128)(2,1)}), bf16[16,16,256]{2,1,0:T(8,128)(2,1)S(1)}, u32[]{:S(2)}, u32[]{:S(2)}) async-start(bf16[16,16,256]{2,1,0:T(8,128)(2,1)} %broadcast_in_dim.2), calls=%async_computation.1 | async-start | bytes 262144 | tf_op jit(solution)/shard_map/all_to_all | solution.py:38
  211.5 84.5 %all-gather.8.cloned.1.call-start = ((), (), s32[]{:S(2)}) async-start(), calls=%async_computation.4 | async-start | bytes 2228224 | tf_op jit(solution)/shard_map/all_gather | solution.py:20
Sparse Core Ops, SparseCore 0:
  11.6 71.1 all-gather.3
  84.8 95.3 all-gather.5
  241.1 54.8 all-gather.7
where the time goes:
time: 307 us
  waiting for transfers between devices  229 us (75%)
  blocking collectives  33.8 us (11%)
  between operations  15.4 us (5%)
  matrix products  11.8 us (4%)
  local copies, waits for them, and re-layouts  9.34 us (3%)
  starting transfers between devices  4.88 us (2%)
    all_gather x2, waiting for transfers between devices, in_one_piece(): out = lax.all_gather(both, axis, axis=dim, tiled=True)  124 us
    all_gather x1, waiting for transfers between devices, body(): inputs = lax.all_gather(saved_input, 'tp', axis=1, tiled=True)  97.5 us
    psum x2, blocking collectives, by_axis(): x = lax.psum(x, axis)  19 us
    all_to_all x1, blocking collectives, sent_and_summed(): pieces = lax.all_to_all(cut_along(x, dim, count), axis, 0, 0, tiled=True)  14.8 us
    dot_general x1, matrix products, body(): query_low = jnp.dot(inputs, bases[0], preferred_element_type=jnp.float32)  6.54 us
    all_to_all x1, waiting for transfers between devices, sent_to_all(): lax.all_to_all(jnp.broadcast_to(x[None], (count, *x.shape)), axis, 0, 0,...  6.45 us
    unnamed x32, local copies, waits for them, and re-layouts  6.25 us
  transfers between devices with their start and end apart: 4, of which 4 were waited for; matrix products, arithmetic and copies ran while one was open for 1% of the time, Pallas kernels for 0%

commit v1 on v0

--- a/solution.py
+++ b/solution.py
@@ -3,6 +3,7 @@
 from jax import lax
 from jax.sharding import Mesh
 from jax.sharding import PartitionSpec as P
+from jax.lax import all_gather
 
 D = 4096
 HD = 128
@@ -104,7 +105,7 @@
     width = query_cot.shape[1]
     low_count = query_first.shape[0]
     cotangents = jnp.concatenate([query_cot, key_cot], axis=1)
-    inputs = lax.all_gather(saved_input, "tp", axis=1, tiled=True)
+    inputs = jnp.concatenate(all_gather(saved_input, axis_name="tp"), 1)
     bases = in_one_piece((query_basis, key_basis), FS, 0, 1)
     query_low = jnp.dot(inputs, bases[0], preferred_element_type=jnp.float32)
     key_low = jnp.dot(inputs, bases[1], preferred_element_type=jnp.float32)

time: 307 us -> 291 us (0.948)
  waiting for transfers between devices: 229 us -> 203 us
  local copies, waits for them, and re-layouts: 9.34 us -> 20.8 us
    all_gather x1, waiting for transfers between devices: 97.5 us -> 83.7 us  [body(): inputs = jnp.concatenate(all_gather(saved_input, axis_name='tp'), 1)]
    all_gather x2, waiting for transfers between devices: 124 us -> 112 us  [in_one_piece(): out = lax.all_gather(both, axis, axis=dim, tiled=True)]
    reshape x0 -> x1, local copies, waits for them, and re-layouts: none -> 11.5 us  [body(): inputs = jnp.concatenate(all_gather(saved_input, axis_name='tp'), 1)]
  transfers between devices with their start and end apart: 4 -> 4, of which waited for: 4 -> 4; matrix products, arithmetic and copies ran while one was open for 1% -> 6% of each run, Pallas kernels for 0% -> 0%
where the time goes in v1:
time: 291 us; the launch traced here: 290 us
  waiting for transfers between devices  203 us (70%)
  blocking collectives  31.8 us (11%)
  local copies, waits for them, and re-layouts  20.8 us (7%)
  between operations  15.4 us (5%)
  matrix products  11.8 us (4%)
  starting transfers between devices  4.88 us (2%)
    all_gather x2, waiting for transfers between devices, in_one_piece(): out = lax.all_gather(both, axis, axis=dim, tiled=True)  112 us
    all_gather x1, waiting for transfers between devices, body(): inputs = jnp.concatenate(all_gather(saved_input, axis_name='tp'), 1)  83.7 us
    psum x2, blocking collectives, by_axis(): x = lax.psum(x, axis)  19 us
    all_to_all x1, blocking collectives, sent_and_summed(): pieces = lax.all_to_all(cut_along(x, dim, count), axis, 0, 0, tiled=True)  12.8 us
    reshape x1, local copies, waits for them, and re-layouts, body(): inputs = jnp.concatenate(all_gather(saved_input, axis_name='tp'), 1)  11.5 us
    dot_general x1, matrix products, body(): query_low = jnp.dot(inputs, bases[0], preferred_element_type=jnp.float32)  6.52 us
    all_to_all x1, waiting for transfers between devices, sent_to_all(): lax.all_to_all(jnp.broadcast_to(x[None], (count, *x.shape)), axis, 0, 0,...  6.45 us
    unnamed x32, local copies, waits for them, and re-layouts  6.26 us
  transfers between devices with their start and end apart: 4, of which 4 were waited for; matrix products, arithmetic and copies ran while one was open for 6% of the time, Pallas kernels for 0%

profile of v1, /device:TPU:2, one launch (start us, length us, event | category | flops | bytes accessed | tf_op | source)
XLA Modules:
  0.0 289.9 jit_solution(745959100085935350)
XLA Ops:
  7.2 0.7 all-gather.9.cloned.1.call-update
  8.0 1.7 pad_maximum_fusion
  9.7 83.7 %all-gather.9.cloned.1.call-done = bf16[32768,128]{1,0:T(8,128)(2,1)} async-done(((bf16[1024,128]{1,0:T(8,128)(2,1)}), bf16[32768,128]{1,0:T(8,128)(2,1)}) %all-gather.9.cloned.1.call-update) | async-done | bytes 8388624 | tf_op jit(solution)/shard_map/all_gather | solution.py:108
  93.4 11.5 %copy.38 = bf16[1024,32,128]{0,2,1:T(8,128)(2,1)} copy(bf16[1024,32,128]{2,0,1:T(8,128)(2,1)} %bitcast.30) | data formatting | bytes 16777216 | tf_op jit(solution)/shard_map/reshape | solution.py:108
  104.8 55.4 %all-gather.5.cloned.1.call-done = bf16[4096,512]{1,0:T(8,128)(2,1)} async-done(((bf16[256,512]{1,0:T(8,128)(2,1)}), bf16[4096,512]{1,0:T(8,128)(2,1)}) %all-gather.5.cloned.1.call-update) | async-done | bytes 4194320 | tf_op jit(solution)/shard_map/all_gather | solution.py:21
  160.3 6.5 %fusion.4 = f32[1024,256]{0,1:T(8,128)S(1)} fusion(bf16[1024,4096]{0,1:T(8,128)(2,1)} %bitcast.28, bf16[4096,512]{1,0:T(8,128)(2,1)} %all-gather.5.cloned.1.call-done), kind=kOutput, calls=%fused_computation.4 | convolution fusion | flops 2147483648 | bytes 11534336 | tf_op jit(solution)/shard_map/dot_general | solution.py:110
  166.8 0.3 fusion.14
  167.2 0.3 convolution_add_fusion.1
  167.5 0.4 copy-done.2
  167.9 2.3 fusion.7
  170.3 0.3 fusion.11
  170.7 0.3 convolution_add_fusion
  171.0 0.1 copy.39
  171.1 12.8 %all_to_all.10 = f32[16,16,256]{2,1,0:T(8,128)S(1)} all-to-all(f32[16,16,256]{2,1,0:T(8,128)S(1)} %bitcast.31), channel_id=1, replica_groups=mesh['fs_0'=4,'fs_1'=4,'tp'=32] {'fs_0','fs_1'}, dimensions={0} | all-to-all | bytes 524288 | tf_op jit(solution)/shard_map/all_to_all | solution.py:33
  184.1 0.7 broadcast_in_dim.2
  184.7 4.8 %all-to-all-start.1 = ((bf16[16,16,256]{2,1,0:T(8,128)(2,1)}), bf16[16,16,256]{2,1,0:T(8,128)(2,1)S(1)}, u32[]{:S(2)}, u32[]{:S(2)}) async-start(bf16[16,16,256]{2,1,0:T(8,128)(2,1)} %broadcast_in_dim.2), calls=%async_computation.1 | async-start | bytes 262144 | tf_op jit(solution)/shard_map/all_to_all | solution.py:39
  189.6 0.1 copy.40
  189.8 6.4 %all-to-all-done.1 = bf16[16,16,256]{2,1,0:T(8,128)(2,1)S(1)} async-done(((bf16[16,16,256]{2,1,0:T(8,128)(2,1)}), bf16[16,16,256]{2,1,0:T(8,128)(2,1)S(1)}, u32[]{:S(2)}, u32[]{:S(2)}) %all-to-all-start.1) | async-done | bytes 131104 | tf_op jit(solution)/shard_map/all_to_all | solution.py:39
  196.2 0.8 multiply_reduce_fusion
  197.0 0.8 multiply_reduce_fusion.1
  197.9 9.2 %all-reduce.1 = (f32[1]{0:T(128)}, f32[1]{0:T(128)}) all-reduce(f32[1]{0:T(128)} %bitcast.7, f32[1]{0:T(128)} %bitcast.10), channel_id=1, replica_groups=mesh['fs_0'=4,'fs_1'=4,'tp'=32] {'fs_0'}, use_global_device_ids=true, to_apply=%region_2.0 | all-reduce | flops 2 | bytes 16 | tf_op jit(solution)/shard_map/psum | solution.py:55
  207.0 9.8 %all-reduce = (f32[1]{0:T(128)}, f32[1]{0:T(128)}) all-reduce(f32[1]{0:T(128)} %get-tuple-element.42, f32[1]{0:T(128)} %get-tuple-element.43), channel_id=1, replica_groups=mesh['fs_0'=4,'fs_1'=4,'tp'=32] {'fs_1'}, use_global_device_ids=true, to_apply=%region_3.0 | all-reduce | flops 2 | bytes 16 | tf_op jit(solution)/shard_map/psum | solution.py:55
  218.3 0.7 pad_maximum_fusion.2
  219.0 0.6 fusion.27
  219.6 0.8 copy.43
  220.3 0.8 copy.42
  221.1 0.8 copy.46
  221.9 0.8 copy.45
  222.6 56.5 %all-gather.7.cloned.1.call-done = bf16[4096,256]{0,1:T(8,128)(2,1)} async-done(((bf16[256,256]{0,1:T(8,128)(2,1)}), bf16[4096,256]{0,1:T(8,128)(2,1)}) %all-gather.7.cloned.1.call-update) | async-done | bytes 2097168 | tf_op jit(solution)/shard_map/all_gather | solution.py:21
  279.1 1.7 fusion.26
  280.8 1.3 copy.47
  282.1 1.3 copy.44
  (33 shorter events, 0.4 us)
Async XLA Ops:
  7.2 159.6 %copy-start = (bf16[1024,128]{1,0:T(8,128)(2,1)S(1)}, bf16[1024,128]{1,0:T(8,128)(2,1)}, u32[]{:S(2)}) copy-start(bf16[1024,128]{1,0:T(8,128)(2,1)} %param.12) | copy-start | bytes 786436
  7.2 86.2 %all-gather.9.cloned.1.call-start = ((), (), s32[]{:S(2)}) async-start(), calls=%async_computation.4 | async-start | bytes 8650752 | tf_op jit(solution)/shard_map/all_gather | solution.py:108
  7.9 152.4 %all-gather.5.cloned.1.call-start = ((), (), s32[]{:S(2)}) async-start(), calls=%async_computation.2 | async-start | bytes 4456448 | tf_op jit(solution)/shard_map/all_gather | solution.py:21
  160.3 7.2 %copy-start.1 = (bf16[1024,32,128]{0,2,1:T(8,128)(2,1)S(1)}, bf16[1024,32,128]{0,2,1:T(8,128)(2,1)}, u32[]{:S(2)}) copy-start(bf16[1024,32,128]{0,2,1:T(8,128)(2,1)} %copy.38) | copy-start | bytes 25165828
  160.3 7.6 %copy-start.2 = (bf16[4096,512]{1,0:T(8,128)(2,1)S(1)}, bf16[4096,512]{1,0:T(8,128)(2,1)}, u32[]{:S(2)}) copy-start(bf16[4096,512]{1,0:T(8,128)(2,1)} %all-gather.5.cloned.1.call-done) | copy-start | bytes 12582916
  167.9 2.3 copy-start.3
  170.2 13.8 %copy-start.8 = (f32[16,128]{1,0:T(8,128)S(1)}, f32[16,128]{1,0:T(8,128)}, u32[]{:S(2)}) copy-start(f32[16,128]{1,0:T(8,128)} %param.21) | copy-start | bytes 24580
  170.2 13.8 %copy-start.9 = (f32[16,128]{1,0:T(8,128)S(1)}, f32[16,128]{1,0:T(8,128)}, u32[]{:S(2)}) copy-start(f32[16,128]{1,0:T(8,128)} %param.19) | copy-start | bytes 24580
  170.3 13.8 %copy-start.10 = (f32[16,128]{1,0:T(8,128)S(1)}, f32[16,128]{1,0:T(8,128)}, u32[]{:S(2)}) copy-start(f32[16,128]{1,0:T(8,128)} %param.20) | copy-start | bytes 24580
  170.3 13.8 %copy-start.11 = (f32[16,128]{1,0:T(8,128)S(1)}, f32[16,128]{1,0:T(8,128)}, u32[]{:S(2)}) copy-start(f32[16,128]{1,0:T(8,128)} %param.18) | copy-start | bytes 24580
  170.3 19.3 %copy-start.6 = (f32[256,128]{1,0:T(8,128)S(1)}, f32[256,128]{1,0:T(8,128)}, u32[]{:S(2)}) copy-start(f32[256,128]{1,0:T(8,128)} %param.14) | copy-start | bytes 393220
  170.3 19.4 %copy-start.7 = (f32[256,128]{1,0:T(8,128)S(1)}, f32[256,128]{1,0:T(8,128)}, u32[]{:S(2)}) copy-start(f32[256,128]{1,0:T(8,128)} %param.15) | copy-start | bytes 393220
  170.3 25.9 %copy-start.4 = (bf16[256,256]{1,0:T(8,128)(2,1)S(1)}, bf16[256,256]{1,0:T(8,128)(2,1)}, u32[]{:S(2)}) copy-start(bf16[256,256]{1,0:T(8,128)(2,1)} %param.17) | copy-start | bytes 393220
  170.3 26.7 %copy-start.5 = (bf16[256,256]{1,0:T(8,128)(2,1)S(1)}, bf16[256,256]{1,0:T(8,128)(2,1)}, u32[]{:S(2)}) copy-start(bf16[256,256]{1,0:T(8,128)(2,1)} %param.16) | copy-start | bytes 393220
  184.7 11.5 %all-to-all-start.1 = ((bf16[16,16,256]{2,1,0:T(8,128)(2,1)}), bf16[16,16,256]{2,1,0:T(8,128)(2,1)S(1)}, u32[]{:S(2)}, u32[]{:S(2)}) async-start(bf16[16,16,256]{2,1,0:T(8,128)(2,1)} %broadcast_in_dim.2), calls=%async_computation.1 | async-start | bytes 262144 | tf_op jit(solution)/shard_map/all_to_all | solution.py:39
  189.5 89.6 %all-gather.7.cloned.1.call-start = ((), (), s32[]{:S(2)}) async-start(), calls=%async_computation.3 | async-start | bytes 2228224 | tf_op jit(solution)/shard_map/all_gather | solution.py:21
Sparse Core Ops, SparseCore 0:
  10.1 83.2 all-gather.8
  97.0 63.2 all-gather.4
  219.1 59.9 all-gather.6
